TPU v7x, 32 devices: a whole 2x2x4 slice. The times are simulated.
32 devices in a mesh: gr: 2 (over x), sp: 8 (over z, y), tp: 2 (over core).
Axes of the slice: x: 2, y: 2, z: 4, core: 2. Of those that a mesh axis runs over, the one named last changes fastest.
Arguments:
- tokens: bfloat16 [8, 1024, 4096], P('gr', 'sp'), parts along dimension 0, may hold values from -6 to 6
- key_weight: bfloat16 [4096, 2048], P('sp', 'tp'), may hold values from -0.09375 to 0.09375
- value_weight: bfloat16 [4096, 2048], P('sp', 'tp'), may hold values from -0.09375 to 0.09375
- log_decay: float32 [32, 8, 1024], P('tp', 'gr', 'sp'), parts along dimension 1, may hold values from -1 to 0, as said below
- new_query: bfloat16 [8, 2048], P('gr', 'tp'), parts along dimension 0, may hold values from -6 to 6
- new_key: bfloat16 [8, 2048], P('gr', 'tp'), parts along dimension 0, may hold values from -24 to 24
- new_value: bfloat16 [8, 2048], P('gr', 'tp'), parts along dimension 0, may hold values from -6 to 6
- step_decay: float32 [32, 8], P('tp', 'gr'), parts along dimension 1, may hold values from -1.5 to -0.05
- norm_gain: float32 [2048], P('tp'), may hold values from 0.1 to 1.9
Outputs:
- state_cache: float32 [512, 32, 64], P('gr', 'tp'), parts along dimension 0
- first_read: bfloat16 [8, 2048], P('gr', 'tp'), parts along dimension 0
There are 2 independent parts, one for each index of `gr`. A program takes and returns all parts, laid end to end along the dimension named above; an argument that names none is the same for every part. Nothing has to cross between parts.
Inputs may be any that keep to these rules, and one draw needn't show every extreme that they name: `log_decay`: every entry is at most zero.
All inputs are finite; a program needn't handle non-finite values.
Results may differ from a plain program's by a relative error of at most 0.0053.
Values may be sent and summed in bfloat16 or wider, within the bound.
A program may use at most 64 MiB of HBM per device.

v0:
```python
import jax
import jax.numpy as jnp
from jax import lax
from jax.sharding import PartitionSpec as P

HEAD_DIM = 64


def entering(x, axis, combine, identity):
    devices, mine = (lax.axis_size(axis), lax.axis_index(axis))
    everything = lax.all_gather(x, axis)
    start = jnp.broadcast_to(jnp.asarray(identity, x.dtype), x.shape)

    def lap(k, before):
        at = devices - 1 - k
        reached = at > mine
        new = combine(before, everything[at])
        return jnp.where(reached, new, before)

    return lax.fori_loop(0, devices, lap, start)


def rotate_half(values, positions):
    half = values.shape[-1] // 2
    inverse = 10000.0 ** (-jnp.arange(half, dtype=jnp.float32) * (2.0 / values.shape[-1]))
    angles = positions[..., None] * inverse
    cosine = jnp.cos(angles)
    sine = jnp.sin(angles)
    first, second = (values[..., :half], values[..., half:])
    return jnp.concatenate(
        [first * cosine - second * sine, second * cosine + first * sine], axis=-1
    )


def add_totals(earlier, later):
    return earlier + later


def shards(
    tokens,
    key_weight,
    value_weight,
    log_decay,
    new_query,
    new_key,
    new_value,
    step_decay,
    norm_gain,
):
    seqs, span, width = tokens.shape
    heads_here = key_weight.shape[1] // HEAD_DIM
    token_rows = tokens.reshape(seqs * span, width)
    whole_keys, whole_values = (
        lax.all_gather(key_weight, "sp", axis=0, tiled=True),
        lax.all_gather(value_weight, "sp", axis=0, tiled=True),
    )
    key_sum = jnp.dot(token_rows, whole_keys, preferred_element_type=jnp.float32)
    value_sum = jnp.dot(token_rows, whole_values, preferred_element_type=jnp.float32)
    key_vectors = (
        lax.optimization_barrier(key_sum.astype(jnp.bfloat16))
        .astype(jnp.float32)
        .reshape(seqs, span, heads_here, HEAD_DIM)
    )
    values = (
        lax.optimization_barrier(value_sum.astype(jnp.bfloat16))
        .astype(jnp.float32)
        .reshape(seqs, span, heads_here, HEAD_DIM)
    )
    devices = lax.axis_size("sp")
    offset = lax.axis_index("sp") * span
    positions = (offset + jnp.arange(span, dtype=jnp.int32)).astype(jnp.float32)
    rkeys = rotate_half(key_vectors, positions[None, :, None]) * HEAD_DIM ** (-0.5)
    totals = jnp.sum(log_decay, axis=-1)
    later_sum = entering(totals, "sp", add_totals, jnp.zeros_like(totals))
    weight = jnp.exp(totals[:, :, None] - jnp.cumsum(log_decay, axis=-1) + later_sum[:, :, None])
    weighted = rkeys * jnp.transpose(weight, (1, 2, 0))[:, :, :, None]
    term = jnp.einsum("stha,sthb->sahb", weighted, values, precision=lax.Precision.HIGHEST)
    term = term.reshape(seqs * HEAD_DIM, heads_here, HEAD_DIM)
    end_pos = jnp.full((seqs, heads_here), float(span * devices), jnp.float32)
    query = rotate_half(new_query.astype(jnp.float32).reshape(seqs, heads_here, HEAD_DIM), end_pos)
    key_new = rotate_half(
        new_key.astype(jnp.float32).reshape(seqs, heads_here, HEAD_DIM), end_pos
    ) * HEAD_DIM ** (-0.5)
    value_new = new_value.astype(jnp.float32).reshape(seqs, heads_here, HEAD_DIM)
    decay_all = jnp.repeat(jnp.exp(step_decay).T, HEAD_DIM, axis=0)
    key_all = jnp.transpose(key_new, (0, 2, 1)).reshape(seqs * HEAD_DIM, heads_here)
    value_all = jnp.repeat(value_new, HEAD_DIM, axis=0)
    summed = lax.psum(term, "sp")
    state_cache = decay_all[:, :, None] * summed + key_all[:, :, None] * value_all
    state_seq = state_cache.reshape(seqs, HEAD_DIM, heads_here, HEAD_DIM)
    raw = jnp.einsum("sha,sahb->shb", query, state_seq, precision=lax.Precision.HIGHEST)
    center = jnp.mean(raw, axis=-1, keepdims=True)
    spread = jnp.mean(jnp.square(raw - center), axis=-1, keepdims=True)
    normed = (raw - center) * lax.rsqrt(spread + 1e-06) * norm_gain.reshape(heads_here, HEAD_DIM)
    first_read = normed.reshape(seqs, heads_here * HEAD_DIM).astype(jnp.bfloat16)
    return (state_cache, first_read)


def solution(mesh):
    placed = (
        P("gr", "sp", None),
        P("sp", "tp"),
        P("sp", "tp"),
        P("tp", "gr", "sp"),
        P("gr", "tp"),
        P("gr", "tp"),
        P("gr", "tp"),
        P("tp", "gr"),
        P("tp"),
    )
    return jax.shard_map(
        shards,
        mesh=mesh,
        in_specs=placed,
        out_specs=(P("gr", "tp", None), P("gr", "tp")),
        check_vma=False,
    )
```

profile of v0, /device:TPU:0, one launch (start us, length us, event | category | flops | bytes accessed | tf_op | source)
XLA Modules:
  0.0 378.3 jit_solution(3645071348651051041)
XLA Ops:
  7.2 0.7 all-gather.7.cloned.1.call-update
  8.0 0.7 all-gather.5.cloned.1.call-update
  9.0 1.1 reduce_window_sum.13
  10.1 28.8 %all-gather.1 = f32[8,16,4]{1,2,0:T(4,128)S(1)} all-gather(f32[1,16,4]{1,2,0:T(4,128)S(1)} %bitcast.52), channel_id=2, replica_groups=mesh['gr'=2,'sp'=8,'tp'=2] {'sp'}, dimensions={0}, use_global_device_ids=true | all-gather | bytes 2304 | tf_op jit(solution)/shard_map/all_gather | solution.py:11
  38.9 0.3 while.16
  39.2 0.1 fusion.13
  39.4 0.1 multiply_cosine_fusion
  39.5 98.0 %all-gather.7.cloned.1.call-done = bf16[4096,1024]{1,0:T(8,128)(2,1)} async-done(((bf16[512,1024]{1,0:T(8,128)(2,1)}), bf16[4096,1024]{1,0:T(8,128)(2,1)}) %all-gather.7.cloned.1.call-update) | async-done | bytes 8388624 | tf_op jit(solution)/shard_map/all_gather | solution.py:54
  137.5 9.1 %convolution_convert_fusion = bf16[512,1024]{1,0:T(8,128)(2,1)S(1)} fusion(bf16[512,4096]{1,0:T(8,128)(2,1)} %bitcast.53, bf16[4096,1024]{1,0:T(8,128)(2,1)} %all-gather.7.cloned.1.call-done), kind=kOutput, calls=%fused_computation.8 | convolution fusion | flops 4295491584 | bytes 13631488 | tf_op jit(solution)/shard_map/dot_general | solution.py:57
  146.6 115.7 %all-gather.5.cloned.1.call-done = bf16[4096,1024]{1,0:T(8,128)(2,1)} async-done(((bf16[512,1024]{1,0:T(8,128)(2,1)}), bf16[4096,1024]{1,0:T(8,128)(2,1)}) %all-gather.5.cloned.1.call-update) | async-done | bytes 8388624 | tf_op jit(solution)/shard_map/all_gather | solution.py:55
  262.3 10.1 %convolution_convert_fusion.1 = bf16[512,1024]{1,0:T(8,128)(2,1)} fusion(bf16[512,4096]{1,0:T(8,128)(2,1)} %bitcast.54, bf16[4096,1024]{1,0:T(8,128)(2,1)} %all-gather.5.cloned.1.call-done), kind=kOutput, calls=%fused_computation.9 | convolution fusion | flops 4295491584 | bytes 13631488 | tf_op jit(solution)/shard_map/dot_general | solution.py:58
  272.4 2.9 reshape.171
  275.4 1.7 copy.30
  277.0 2.9 reshape.158
  279.9 2.1 multiply_subtract_fusion
  282.1 0.6 maximum_multiply_fusion
  282.7 2.1 fusion.5
  284.7 1.4 copy.37
  286.2 2.1 reshape.148
  288.6 0.1 mul.185
  288.9 0.1 multiply_subtract_fusion.1
  289.2 0.2 copy.45
  289.4 1.2 broadcast_in_dim.8
  290.6 1.1 reshape.153
  291.9 73.2 %all-reduce.2.cloned.1.call-done = f32[256,16,64]{0,2,1:T(8,128)} async-done(((f32[256,16,64]{0,2,1:T(8,128)}), f32[256,16,64]{0,2,1:T(8,128)}) %all-reduce.2.cloned.1.call-update) | async-done | bytes 1048592 | tf_op jit(solution)/shard_map/psum | solution.py:88
  365.0 1.4 multiply_add_fusion
  366.4 0.9 reshape.156
  367.3 3.4 fusion.2
  370.7 0.1 reduce_sum.28
  370.8 0.2 multiply_reduce_fusion
  371.0 0.1 multiply_convert_fusion
  371.1 0.7 convert_element_type.28
  (47 shorter events, 1.3 us)
Async XLA Ops:
  7.2 1.6 copy-start.1
  7.2 130.3 %all-gather.7.cloned.1.call-start = ((), (), s32[]{:S(2)}) async-start(), calls=%async_computation.1 | async-start | bytes 9437184 | tf_op jit(solution)/shard_map/all_gather | solution.py:54
  7.9 254.4 %all-gather.5.cloned.1.call-start = ((), (), s32[]{:S(2)}) async-start(), calls=%async_computation | async-start | bytes 9437184 | tf_op jit(solution)/shard_map/all_gather | solution.py:55
  8.7 356.3 %all-reduce.2.cloned.1.call-start = ((), (), s32[]{:S(2)}) async-start(), calls=%async_computation.2 | async-start | bytes 2097152 | tf_op jit(solution)/shard_map/psum | solution.py:88
  286.2 2.2 copy-start.6
  286.2 2.3 copy-start.5
  286.2 2.5 copy-start.3
  286.2 2.6 copy-start.4
  286.2 3.0 copy-start.2
  366.4 4.3 %copy-start = (f32[256,16,64]{0,2,1:T(8,128)}, f32[256,16,64]{0,2,1:T(8,128)S(1)}, u32[]{:S(2)}) copy-start(f32[256,16,64]{0,2,1:T(8,128)S(1)} %multiply_add_fusion) | copy-start | bytes 3145732
Sparse Core Ops, SparseCore 0:
  10.1 127.3 all-gather.6
  139.6 122.6 all-gather.4
  288.5 76.4 all-reduce.1
where the time goes:
time: 379 us; the launch traced here: 378 us
  waiting for transfers between devices  288 us (76%)
  blocking collectives  28.8 us (8%)
  matrix products  24.7 us (7%)
  local copies, waits for them, and re-layouts  16 us (4%)
  between operations  14 us (4%)
  other arithmetic  6.37 us (2%)
    all_gather x1, waiting for transfers between devices, shards(): lax.all_gather(value_weight, 'sp', axis=0, tiled=True)  116 us
    all_gather x1, waiting for transfers between devices, shards(): lax.all_gather(key_weight, 'sp', axis=0, tiled=True)  98 us
    psum x1, waiting for transfers between devices, shards(): summed = lax.psum(term, 'sp')  73.2 us
    all_gather x1, blocking collectives, entering(): everything = lax.all_gather(x, axis)  28.8 us
    dot_general x1, matrix products, shards(): jnp.dot(token_rows, whole_values, preferred_element_type=jnp.float32)  10.1 us
    dot_general x1, matrix products, shards(): jnp.dot(token_rows, whole_keys, preferred_element_type=jnp.float32)  9.14 us
  transfers between devices with their start and end apart: 3, of which 3 were waited for; matrix products, arithmetic and copies ran while one was open for 4% of the time, Pallas kernels for 0%

commit v1 on v0

--- a/solution.py
+++ b/solution.py
@@ -2,8 +2,18 @@
 import jax.numpy as jnp
 from jax import lax
 from jax.sharding import PartitionSpec as P
+from jax.lax import axis_size, ppermute
 
 HEAD_DIM = 64
+
+
+def _meet_sheet(field):
+    nodes = axis_size("sp")
+    high = field
+    for pp in [[(dev, dev ^ d) for dev in range(nodes)] for d in (1, 2, 4, 8, 16) if d < nodes]:
+        top = ppermute(high, "sp", pp)
+        high = high + top
+    return high
 
 
 def entering(x, axis, combine, identity):
@@ -85,7 +95,7 @@
     decay_all = jnp.repeat(jnp.exp(step_decay).T, HEAD_DIM, axis=0)
     key_all = jnp.transpose(key_new, (0, 2, 1)).reshape(seqs * HEAD_DIM, heads_here)
     value_all = jnp.repeat(value_new, HEAD_DIM, axis=0)
-    summed = lax.psum(term, "sp")
+    summed = _meet_sheet(term)
     state_cache = decay_all[:, :, None] * summed + key_all[:, :, None] * value_all
     state_seq = state_cache.reshape(seqs, HEAD_DIM, heads_here, HEAD_DIM)
     raw = jnp.einsum("sha,sahb->shb", query, state_seq, precision=lax.Precision.HIGHEST)

time: 379 us -> 396 us (1.045)
  waiting for transfers between devices: 288 us -> 300 us
    ppermute x0 -> x3, waiting for transfers between devices: none -> 84.8 us  [_meet_sheet(): top = ppermute(high, 'sp', pp)]
    psum x1 -> x0, waiting for transfers between devices: 73.2 us -> none  [shards(): summed = lax.psum(term, 'sp')]
  transfers between devices with their start and end apart: 3 -> 5, of which waited for: 3 -> 5; matrix products, arithmetic and copies ran while one was open for 4% -> 4% of each run, Pallas kernels for 0% -> 0%
where the time goes in v1:
time: 396 us; the launch traced here: 395 us
  waiting for transfers between devices  300 us (76%)
  blocking collectives  28.8 us (7%)
  matrix products  24.7 us (6%)
  local copies, waits for them, and re-layouts  17.7 us (4%)
  between operations  14.3 us (4%)
  other arithmetic  7.11 us (2%)
    all_gather x1, waiting for transfers between devices, shards(): lax.all_gather(value_weight, 'sp', axis=0, tiled=True)  116 us
    all_gather x1, waiting for transfers between devices, shards(): lax.all_gather(key_weight, 'sp', axis=0, tiled=True)  98 us
    ppermute x3, waiting for transfers between devices, _meet_sheet(): top = ppermute(high, 'sp', pp)  84.8 us
    all_gather x1, blocking collectives, entering(): everything = lax.all_gather(x, axis)  28.8 us
    dot_general x1, matrix products, shards(): jnp.dot(token_rows, whole_values, preferred_element_type=jnp.float32)  10.1 us
    dot_general x1, matrix products, shards(): jnp.dot(token_rows, whole_keys, preferred_element_type=jnp.float32)  9.14 us
  transfers between devices with their start and end apart: 5, of which 5 were waited for; matrix products, arithmetic and copies ran while one was open for 4% of the time, Pallas kernels for 0%

profile of v1, /device:TPU:0, one launch (start us, length us, event | category | flops | bytes accessed | tf_op | source)
XLA Modules:
  0.0 395.3 jit_solution(8710993121616879138)
XLA Ops:
  7.2 0.7 all-gather.7.cloned.1.call-update
  8.0 0.7 all-gather.5.cloned.1.call-update
  9.0 1.1 reduce_window_sum.13
  10.1 28.8 %all-gather.1 = f32[8,16,4]{1,2,0:T(4,128)S(1)} all-gather(f32[1,16,4]{1,2,0:T(4,128)S(1)} %bitcast.52), channel_id=2, replica_groups=mesh['gr'=2,'sp'=8,'tp'=2] {'sp'}, dimensions={0}, use_global_device_ids=true | all-gather | bytes 2304 | tf_op jit(solution)/shard_map/all_gather | solution.py:21
  38.9 0.3 while.16
  39.5 98.0 %all-gather.7.cloned.1.call-done = bf16[4096,1024]{1,0:T(8,128)(2,1)} async-done(((bf16[512,1024]{1,0:T(8,128)(2,1)}), bf16[4096,1024]{1,0:T(8,128)(2,1)}) %all-gather.7.cloned.1.call-update) | async-done | bytes 8388624 | tf_op jit(solution)/shard_map/all_gather | solution.py:64
  137.4 9.1 %convolution_convert_fusion = bf16[512,1024]{1,0:T(8,128)(2,1)S(1)} fusion(bf16[512,4096]{1,0:T(8,128)(2,1)} %bitcast.53, bf16[4096,1024]{1,0:T(8,128)(2,1)} %all-gather.7.cloned.1.call-done), kind=kOutput, calls=%fused_computation.8 | convolution fusion | flops 4295491584 | bytes 13631488 | tf_op jit(solution)/shard_map/dot_general | solution.py:67
  146.6 115.7 %all-gather.5.cloned.1.call-done = bf16[4096,1024]{1,0:T(8,128)(2,1)} async-done(((bf16[512,1024]{1,0:T(8,128)(2,1)}), bf16[4096,1024]{1,0:T(8,128)(2,1)}) %all-gather.5.cloned.1.call-update) | async-done | bytes 8388624 | tf_op jit(solution)/shard_map/all_gather | solution.py:65
  262.3 10.1 %convolution_convert_fusion.1 = bf16[512,1024]{1,0:T(8,128)(2,1)} fusion(bf16[512,4096]{1,0:T(8,128)(2,1)} %bitcast.54, bf16[4096,1024]{1,0:T(8,128)(2,1)} %all-gather.5.cloned.1.call-done), kind=kOutput, calls=%fused_computation.9 | convolution fusion | flops 4295491584 | bytes 13631488 | tf_op jit(solution)/shard_map/dot_general | solution.py:68
  272.4 2.9 reshape.171
  275.3 1.6 copy.30
  277.0 2.9 reshape.158
  279.9 2.1 multiply_subtract_fusion
  282.0 0.6 maximum_multiply_fusion
  282.6 2.1 fusion.5
  284.7 1.4 copy.37
  286.1 1.1 reshape.148
  287.2 0.6 collective-permute-start
  287.8 23.6 %collective-permute-done = f32[256,16,64]{0,2,1:T(8,128)S(1)} collective-permute-done((f32[256,16,64]{0,2,1:T(8,128)S(1)}, f32[256,16,64]{0,2,1:T(8,128)S(1)}, u32[]{:S(2)}, u32[]{:S(2)}) %collective-permute-start) | collective-permute-done | bytes 1048608 | tf_op jit(solution)/shard_map/ppermute | solution.py:14
  311.5 0.2 add.99
  311.8 23.3 %collective-permute-done.1 = f32[256,16,64]{0,2,1:T(8,128)S(1)} collective-permute-done((f32[256,16,64]{0,2,1:T(8,128)S(1)}, f32[256,16,64]{0,2,1:T(8,128)S(1)}, u32[]{:S(2)}, u32[]{:S(2)}) %collective-permute-start.1) | collective-permute-done | bytes 1048608 | tf_op jit(solution)/shard_map/ppermute | solution.py:14
  335.1 0.2 add.100
  335.3 1.9 collective-permute-start.2
  338.0 1.0 copy.45
  339.0 2.2 broadcast_in_dim.8
  341.2 2.1 reshape.153
  343.4 37.9 %collective-permute-done.2 = f32[256,16,64]{0,2,1:T(8,128)} collective-permute-done((f32[256,16,64]{0,2,1:T(8,128)S(1)}, f32[256,16,64]{0,2,1:T(8,128)}, u32[]{:S(2)}, u32[]{:S(2)}) %collective-permute-start.2) | collective-permute-done | bytes 1048608 | tf_op jit(solution)/shard_map/ppermute | solution.py:14
  381.3 1.8 multiply_add_fusion
  383.1 0.9 reshape.156
  384.0 3.4 fusion.2
  387.5 0.2 multiply_reduce_fusion
  387.7 0.7 convert_element_type.28
  (52 shorter events, 1.9 us)
Async XLA Ops:
  7.2 1.5 copy-start.1
  7.2 130.3 %all-gather.7.cloned.1.call-start = ((), (), s32[]{:S(2)}) async-start(), calls=%async_computation.1 | async-start | bytes 9437184 | tf_op jit(solution)/shard_map/all_gather | solution.py:64
  7.9 254.4 %all-gather.5.cloned.1.call-start = ((), (), s32[]{:S(2)}) async-start(), calls=%async_computation | async-start | bytes 9437184 | tf_op jit(solution)/shard_map/all_gather | solution.py:65
  287.2 24.2 %collective-permute-start = (f32[256,16,64]{0,2,1:T(8,128)S(1)}, f32[256,16,64]{0,2,1:T(8,128)S(1)}, u32[]{:S(2)}, u32[]{:S(2)}) collective-permute-start(f32[256,16,64]{0,2,1:T(8,128)S(1)} %reshape.148), channel_id=1, source_target_pairs={{0,2},{2,0},{4,6},{6,4},{8,10},{10,8},{12,14},{14,12},{1,3},{3,1},... | collective-permute-start | bytes 3145736 | tf_op jit(solution)/shard_map/ppermute | solution.py:14
  311.6 25.5 %copy-start.6 = (f32[16,4]{0,1:T(4,128)S(1)}, f32[16,4]{0,1:T(4,128)}, u32[]{:S(2)}) copy-start(f32[16,4]{0,1:T(4,128)} %param.18) | copy-start | bytes 772
  311.6 25.6 %copy-start.5 = (f32[1024]{0:T(1024)S(1)}, f32[1024]{0:T(1024)}, u32[]{:S(2)}) copy-start(f32[1024]{0:T(1024)} %param.19) | copy-start | bytes 12292
  311.7 25.8 %copy-start.3 = (bf16[4,1024]{1,0:T(4,128)(2,1)S(1)}, bf16[4,1024]{1,0:T(4,128)(2,1)}, u32[]{:S(2)}) copy-start(bf16[4,1024]{1,0:T(4,128)(2,1)} %param.15) | copy-start | bytes 24580
  311.7 25.9 %copy-start.4 = (bf16[4,1024]{1,0:T(4,128)(2,1)S(1)}, bf16[4,1024]{1,0:T(4,128)(2,1)}, u32[]{:S(2)}) copy-start(bf16[4,1024]{1,0:T(4,128)(2,1)} %param.16) | copy-start | bytes 24580
  311.7 26.3 %copy-start.2 = (bf16[4,1024]{1,0:T(4,128)(2,1)S(1)}, bf16[4,1024]{1,0:T(4,128)(2,1)}, u32[]{:S(2)}) copy-start(bf16[4,1024]{1,0:T(4,128)(2,1)} %param.17) | copy-start | bytes 24580
  311.7 23.4 %collective-permute-start.1 = (f32[256,16,64]{0,2,1:T(8,128)S(1)}, f32[256,16,64]{0,2,1:T(8,128)S(1)}, u32[]{:S(2)}, u32[]{:S(2)}) collective-permute-start(f32[256,16,64]{0,2,1:T(8,128)S(1)} %add.99), channel_id=1, source_target_pairs={{0,4},{2,6},{4,0},{6,2},{8,12},{10,14},{12,8},{14,10},{1,5},{3,7},... | collective-permute-start | bytes 3145736 | tf_op jit(solution)/shard_map/ppermute | solution.py:14
  335.3 46.0 %collective-permute-start.2 = (f32[256,16,64]{0,2,1:T(8,128)S(1)}, f32[256,16,64]{0,2,1:T(8,128)}, u32[]{:S(2)}, u32[]{:S(2)}) collective-permute-start(f32[256,16,64]{0,2,1:T(8,128)S(1)} %add.100), channel_id=1, source_target_pairs={{0,8},{2,10},{4,12},{6,14},{8,0},{10,2},{12,4},{14,6},{1,9},{3,11}... | collective-permute-start | bytes 3145736 | tf_op jit(solution)/shard_map/ppermute | solution.py:14
  383.1 4.3 %copy-start = (f32[256,16,64]{0,2,1:T(8,128)}, f32[256,16,64]{0,2,1:T(8,128)S(1)}, u32[]{:S(2)}) copy-start(f32[256,16,64]{0,2,1:T(8,128)S(1)} %multiply_add_fusion) | copy-start | bytes 3145732
Sparse Core Ops, SparseCore 0:
  10.1 127.2 all-gather.6
  139.6 122.6 all-gather.4
